TPU v7x, 32 devices: a whole 2x2x4 slice. The times are simulated.
32 devices in a mesh: kv: 8 (over z, y), tp: 4 (over x, core).
Axes of the slice: x: 2, y: 2, z: 4, core: 2. Of those that a mesh axis runs over, the one named last changes fastest.
Arguments:
- hidden: bfloat16 [128, 4096], P(None, 'tp'), may hold values from -50 to 50
- input_gain: bfloat16 [4096], P('tp'), may hold values from 0.099609375 to 1.8984375
- x_weight: bfloat16 [4096, 8192], P('tp', 'kv'), may hold values from -0.09375 to 0.09375
- z_weight: bfloat16 [4096, 8192], P('tp', 'kv'), may hold values from -0.09375 to 0.09375
- bc_weight: bfloat16 [4096, 8192], P('tp', 'kv'), may hold values from -0.09375 to 0.09375
- dt_weight: bfloat16 [4096, 128], P('tp', 'kv'), may hold values from -0.09375 to 0.09375
- x_kernel: bfloat16 [4, 8192], P(None, 'kv'), may hold values from -3 to 3
- bc_kernel: bfloat16 [4, 8192], P(None, 'kv'), may hold values from -3 to 3
- dt_bias: float32 [128], P('kv'), may hold values from -3 to 0.5
- decay_log: float32 [128], P('kv'), may hold values from -3 to 1.5
- skip_scale: float32 [128], P('kv'), may hold values from 0.5 to 1.5
- output_gain: bfloat16 [8192], P('kv'), may hold values from 0.099609375 to 1.8984375
- output_weight: bfloat16 [8192, 4096], P('kv'), may hold values from -0.09375 to 0.09375
- saved_states: float32 [32, 5, 128, 64, 128], P('tp', None, 'kv'), may hold values from -1.8 to 1.8
- x_history: bfloat16 [32, 7, 8192], P('tp', None, 'kv'), may hold values from -6 to 6
- bc_history: bfloat16 [32, 7, 8192], P('tp', None, 'kv'), may hold values from -6 to 6
- accepted: int32 [32], P('tp'), may hold values from 0 to 4
Outputs:
- mixed: bfloat16 [128, 4096], P('tp', 'kv')
- new_states: float32 [32, 5, 128, 64, 128], P('tp', None, 'kv')
- x_window: bfloat16 [32, 7, 8192], P('tp', None, 'kv')
- bc_window: bfloat16 [32, 7, 8192], P('tp', None, 'kv')
All inputs are finite; a program needn't handle non-finite values.
Results may differ from a plain program's by a relative error of at most 0.02.
Values may be sent and summed in bfloat16 or wider, within the bound.
A program may use at most 192 MiB of HBM per device.

v0:
```python
import jax
import jax.numpy as jnp
from jax import lax
from jax.sharding import PartitionSpec as P

D = 4096
PROPS = 4
INNER = 8192


EPSILON = 1e-05


def partner_2(block, axis, stride):
    count = lax.axis_size(axis)
    route = []
    for low in range(count):
        high = low | 1 << stride
        if high != low and high < count:
            route += [(low, high), (high, low)]
    return lax.ppermute(block, axis, route)


def take_window(history, accepted, fresh_rows):
    history_len = history.shape[1] - fresh_rows.shape[1]
    indices = accepted[:, None] + jnp.arange(history_len, dtype=jnp.int32)[None, :]
    kept_rows = jnp.take_along_axis(history, indices[:, :, None], axis=1)
    return jnp.concatenate([kept_rows, fresh_rows], axis=1)


def conv_silu(window, kernel):
    length = window.shape[1] - kernel.shape[0] + 1
    running = window[:, 0:length].astype(jnp.float32) * kernel[0].astype(jnp.float32)
    for offset in range(1, kernel.shape[0]):
        running = running + window[:, offset : offset + length].astype(jnp.float32) * kernel[
            offset
        ].astype(jnp.float32)
    return jax.nn.silu(running)


def ssd_block(x_conv, step_size, decay_rate, b_terms, c_terms, first_state, skip_scale):
    cumulated = jnp.cumsum(-decay_rate * step_size, axis=1)
    length = x_conv.shape[1]
    indices = jnp.arange(length)
    causal = indices[:, None] >= indices[None, :]
    gaps = cumulated[:, :, None, :] - cumulated[:, None, :, :]
    weights = jnp.exp(jnp.where(causal[None, :, :, None], gaps, -jnp.inf))
    inputs = x_conv * step_size[..., None]
    outer_prod = jnp.einsum("srhp,srhn->srhpn", inputs, b_terms)
    states = jnp.exp(cumulated)[..., None, None] * first_state[:, None] + jnp.einsum(
        "strh,srhpn->sthpn", weights, outer_prod
    )
    output = jnp.einsum("sthn,sthpn->sthp", c_terms, states) + skip_scale[:, None] * x_conv
    return (output, states)


def local(
    hidden,
    input_gain,
    x_weight,
    z_weight,
    bc_weight,
    dt_weight,
    x_kernel,
    bc_kernel,
    dt_bias,
    decay_log,
    skip_scale,
    output_gain,
    output_weight,
    saved_states,
    x_history,
    bc_history,
    accepted,
):
    heads_here = dt_bias.shape[0]
    head_size = x_weight.shape[1] // heads_here
    state_size = saved_states.shape[4]
    seqs_here = accepted.shape[0]
    rows_here = hidden.shape[0] // lax.axis_size("tp")
    inner_here = x_weight.shape[1]
    bc_here = bc_weight.shape[1]
    widened = hidden.astype(jnp.float32)
    squares = lax.psum(jnp.sum(widened * widened, axis=1), "tp")
    normed = (
        widened * lax.rsqrt(squares[:, None] / D + EPSILON) * input_gain.astype(jnp.float32)
    ).astype(jnp.bfloat16)
    weights = jnp.concatenate([x_weight, z_weight, bc_weight, dt_weight], axis=1)
    product = jnp.dot(normed, weights, preferred_element_type=jnp.float32)
    projected = lax.psum_scatter(
        lax.optimization_barrier(product.astype(jnp.bfloat16))
        .astype(jnp.float32)
        .astype(jnp.bfloat16),
        "tp",
        scatter_dimension=0,
        tiled=True,
    )
    x_fresh = projected[:, :inner_here]
    z_fresh = projected[:, inner_here : 2 * inner_here]
    bc_fresh = projected[:, 2 * inner_here : 2 * inner_here + bc_here]
    dt_fresh = projected[:, 2 * inner_here + bc_here :]
    x_window = take_window(x_history, accepted, x_fresh.reshape(seqs_here, PROPS, inner_here))
    bc_window = take_window(bc_history, accepted, bc_fresh.reshape(seqs_here, PROPS, bc_here))
    x_conv = conv_silu(x_window, x_kernel).reshape(seqs_here, PROPS, heads_here, head_size)
    bc_conv = conv_silu(bc_window, bc_kernel)
    spread = max(4 // heads_here, 1)
    position = lax.axis_index("kv")
    for level in range(spread.bit_length() - 1):
        partner = partner_2(bc_conv, "kv", level)
        low_half = position // 2**level % 2 == 0
        bc_conv = jnp.where(
            low_half,
            jnp.concatenate([bc_conv, partner], axis=2),
            jnp.concatenate([partner, bc_conv], axis=2),
        )
    groups_here = bc_conv.shape[2] // (2 * state_size)
    paired = bc_conv.reshape(seqs_here, PROPS, groups_here, 2, state_size)
    per_group = heads_here // groups_here
    b_terms = jnp.repeat(paired[:, :, :, 0], per_group, axis=2)
    c_terms = jnp.repeat(paired[:, :, :, 1], per_group, axis=2)
    step_size = jax.nn.softplus(
        dt_fresh.astype(jnp.float32).reshape(seqs_here, PROPS, heads_here) + dt_bias
    )
    first_state = jnp.take_along_axis(saved_states, accepted[:, None, None, None, None], axis=1)[
        :, 0
    ]
    output, states = ssd_block(
        x_conv, step_size, jnp.exp(decay_log), b_terms, c_terms, first_state, skip_scale
    )
    new_states = jnp.concatenate([first_state[:, None], states], axis=1)
    gate_values = z_fresh.astype(jnp.float32).reshape(seqs_here, PROPS, heads_here, head_size)
    gated = (output * jax.nn.silu(gate_values)).reshape(rows_here, inner_here)
    square_sum = jnp.sum(gated * gated, axis=1)
    scaled = (gated * output_gain.astype(jnp.float32)).astype(jnp.bfloat16)
    partial_value = jnp.dot(scaled, output_weight, preferred_element_type=jnp.float32)
    total_squares = lax.psum(square_sum, "kv")
    summed = lax.psum_scatter(partial_value, "kv", scatter_dimension=1, tiled=True)
    mixed = (lax.rsqrt(total_squares / INNER + EPSILON)[:, None] * summed).astype(jnp.bfloat16)
    return (mixed, new_states, x_window, bc_window)


def solution(mesh):
    in_specs = (
        P(None, "tp"),
        P("tp"),
        P("tp", "kv"),
        P("tp", "kv"),
        P("tp", "kv"),
        P("tp", "kv"),
        P(None, "kv"),
        P(None, "kv"),
        P("kv"),
        P("kv"),
        P("kv"),
        P("kv"),
        P("kv", None),
        P("tp", None, "kv", None, None),
        P("tp", None, "kv"),
        P("tp", None, "kv"),
        P("tp"),
    )
    out_specs = (
        P("tp", "kv"),
        P("tp", None, "kv", None, None),
        P("tp", None, "kv"),
        P("tp", None, "kv"),
    )
    return jax.shard_map(local, mesh=mesh, in_specs=in_specs, out_specs=out_specs, check_vma=False)
```

profile of v0, /device:TPU:0, one launch (start us, length us, event | category | flops | bytes accessed | tf_op | source)
XLA Modules:
  0.0 164.1 jit_solution(15969078561055886669)
XLA Ops:
  7.2 0.0 copy-start
  7.2 0.0 reduce-scatter.7.cloned.1.call-start
  7.2 1.1 fusion.19
  8.3 8.4 %psum.14 = f32[128]{0:T(128)S(1)} all-reduce(f32[128]{0:T(128)S(1)} %fusion.19), channel_id=1, replica_groups=mesh['kv'=8,'tp'=4] {'tp'}, use_global_device_ids=true, to_apply=%region_1.3 | all-reduce | flops 128 | bytes 1024 | tf_op jit(solution)/shard_map/psum | solution.py:84
  16.7 0.7 convert_element_type.130
  17.4 0.9 copy.75
  18.3 0.0 copy-start.11
  18.3 0.0 copy-start.5
  18.4 5.7 %fusion.16 = bf16[128,3088]{0,1:T(8,128)(2,1)S(1)} fusion(bf16[1024,16]{1,0:T(8,128)(2,1)S(1)} %copy.75, bf16[1024,1024]{1,0:T(8,128)(2,1)} %param.23, bf16[1024,1024]{1,0:T(8,128)(2,1)} %param.22, bf16[1024,1024]{1,0:T(8,128)(2,1)} %param.21, bf16[128,1024]{1,0:T(8,128)(2,1)} %param.19, f32[1024]{0:T(1024)S(1)} %convert_element_type.130, ...), kind=kOutput, calls=%fused_computation.20 | convolution fusion | flops 835717120 | bytes 7381504 | tf_op jit(solution)/shard_map/dot_general | solution.py:89
  24.1 1.7 %copy.94 = bf16[128,3088]{1,0:T(8,128)(2,1)} copy(bf16[128,3088]{0,1:T(8,128)(2,1)S(1)} %fusion.16) | data formatting | bytes 1581056
  25.8 0.0 reduce-scatter.7.cloned.1.call-update
  25.8 0.0 reduce-scatter.5.cloned.1.call-start
  26.1 0.1 copy.73
  26.2 0.1 copy.74
  26.3 0.1 reshape.248
  26.4 0.9 gather_fusion.2
  27.3 0.9 gather_fusion.1
  28.2 10.2 %gather_fusion = f32[8,16,64,128]{3,2,1,0:T(8,128)} fusion(f32[8,5,16,64,128]{4,3,2,1,0:T(8,128)} %param.32, s32[8]{0:T(128)S(1)} %or_bitcast_fusion), kind=kCustom, calls=%fused_computation.2 | custom fusion | bytes 8388672 | tf_op jit(solution)/shard_map/jit(take_along_axis)/gather | solution.py:124
  38.4 0.1 broadcast_select_fusion.2
  38.6 5.2 %broadcast_select_fusion.1 = f32[8,16,64,128]{3,2,1,0:T(8,128)} fusion(f32[8,16,64,128]{3,2,1,0:T(8,128)} %gather_fusion, pred[8]{0:T(512)(128)(4,1)S(1)} %compare_and_fusion), kind=kLoop, calls=%fused_computation.21 | loop fusion | flops 1048576 | bytes 8388616 | tf_op jit(solution)/shard_map/jit(take_along_axis)/select_n | solution.py:124
  43.8 6.5 %broadcast_select_fusion = f32[8,1,16,64,128]{4,1,3,2,0:T(1,128)} fusion(f32[8,1,16,64,128]{4,1,3,2,0:T(1,128)S(1)} %bitcast.44, pred[8]{0:T(512)(128)(4,1)S(1)} %compare_and_fusion), kind=kLoop, calls=%fused_computation.11 | loop fusion | flops 1048576 | bytes 8388616 | tf_op jit(solution)/shard_map/jit(take_along_axis)/select_n | solution.py:124
  50.3 0.7 slice.94
  51.1 0.1 copy.84
  51.2 0.1 copy.78
  51.3 0.9 fusion.54
  52.3 0.1 pad_maximum_fusion.1
  52.5 0.7 copy.89
  53.2 0.7 copy.88
  53.9 0.5 divide_multiply_fusion
  54.4 0.2 reshape.210
  54.6 0.1 reshape.204
  54.7 0.1 fusion.55
  54.8 0.1 reshape.226
  54.9 0.1 broadcast_multiply_fusion
  55.1 2.9 %copy.82 = f32[8,4,16,64]{1,3,2,0:T(8,128)} copy(f32[8,4,16,64]{3,2,1,0:T(8,128)S(1)} %broadcast_multiply_fusion) | data formatting | bytes 262144 | tf_op jit(solution)/shard_map/mul | solution.py:48
  58.0 15.6 %bitcast_add_fusion = f32[8,4,16,64,128]{4,1,3,2,0:T(4,128)S(1)} fusion(f32[8,4,16,128]{3,1,2,0:T(4,128)S(1)} %bitcast.45, f32[8,4,16,64]{1,3,2,0:T(8,128)} %copy.82, f32[8,16,64,128]{3,2,1,0:T(8,128)} %broadcast_select_fusion.1, f32[8,4,16]{1,2,0:T(8,128)S(1)} %copy.78, f32[8,4,16]{1,2,0:T(8,128)S(1)} %copy.84, pred[4,4]{1,0:T(4,128)(4,1)S(1)} %iota_compare_fusion), kind=kOutput, calls=%fused_computation.4 | convolution fusion | flops 46141440 | bytes 21368848 | tf_op jit(solution)/shard_map/strh,srhpn->sthpn/dot_general | solution.py:50
  73.8 6.1 %copy-done.3 = f32[8,4,16,64,128]{4,1,3,2,0:T(4,128)} copy-done((f32[8,4,16,64,128]{4,1,3,2,0:T(4,128)}, f32[8,4,16,64,128]{4,1,3,2,0:T(4,128)S(1)}, u32[]{:S(2)}) %copy-start.3) | copy-done | bytes 16777240
  79.8 5.1 %fusion = f32[8,4,16,1,64]{4,3,2,1,0:T(1,128)} fusion(f32[8,4,16,128,1]{3,4,2,1,0:T(1,128)S(1)} %bitcast.46, f32[8,4,16,64,128]{4,1,3,2,0:T(4,128)S(1)} %bitcast_add_fusion), kind=kOutput, calls=%fused_computation.5 | convolution fusion | flops 8388608 | bytes 17170432 | tf_op jit(solution)/shard_map/sthn,sthpn->sthp/dot_general | solution.py:53
  85.0 1.2 multiply_reduce_fusion
  86.2 0.1 reduce_sum.22
  86.3 0.1 reshape.214
  86.4 5.7 %fusion.33 = f32[32,4096]{1,0:T(8,128)} fusion(bf16[1024,4096]{1,0:T(8,128)(2,1)} %param.31, f32[32,1024]{1,0:T(8,128)S(1)} %reshape.214, f32[1024]{0:T(1024)S(1)} %convert_element_type.157), kind=kOutput, calls=%fused_computation.57 | convolution fusion | flops 268500992 | bytes 9048064 | tf_op jit(solution)/shard_map/dot_general | solution.py:135
  92.1 0.0 reduce-scatter.5.cloned.1.call-update
  92.2 20.0 %pad_maximum_fusion = f32[8,5,16,64,128]{4,1,3,2,0:T(8,128)} fusion(f32[8,4,16,64,128]{4,1,3,2,0:T(4,128)} %copy-done.3, f32[8,1,16,64,128]{4,1,3,2,0:T(1,128)} %broadcast_select_fusion), kind=kLoop, calls=%fused_computation.3 | loop fusion | flops 5242880 | bytes 41943040 | tf_op jit(solution)/shard_map/concatenate | solution.py:130
  112.2 19.5 %copy.87 = f32[8,5,16,64,128]{4,3,2,1,0:T(8,128)} copy(f32[8,5,16,64,128]{4,1,3,2,0:T(8,128)} %pad_maximum_fusion) | data formatting | bytes 41943040
  131.6 21.9 %psum.15 = f32[32]{0:T(128)S(1)} all-reduce(f32[32]{0:T(128)S(1)} %reduce_sum.22), channel_id=1, replica_groups=mesh['kv'=8,'tp'=4] {'kv'}, use_global_device_ids=true, to_apply=%region_5.7 | all-reduce | flops 32 | bytes 256 | tf_op jit(solution)/shard_map/psum | solution.py:136
  153.5 2.3 %reduce-scatter.5.cloned.1.call-done = f32[32,512]{1,0:T(8,128)} async-done(((f32[32,4096]{1,0:T(8,128)}), f32[32,512]{1,0:T(8,128)}) %reduce-scatter.5.cloned.1.call-update) | async-done | bytes 65552 | tf_op jit(solution)/shard_map/reduce_scatter | solution.py:137
  155.8 1.5 multiply_convert_fusion.2
  (45 shorter events, 0.5 us)
Async XLA Ops:
  7.2 19.2 %copy-start = (bf16[8,7,1024]{2,0,1:T(8,128)(2,1)S(1)}, bf16[8,7,1024]{2,0,1:T(8,128)(2,1)}, u32[]{:S(2)}) copy-start(bf16[8,7,1024]{2,0,1:T(8,128)(2,1)} %param.33) | copy-start | bytes 344068
  7.2 43.1 %reduce-scatter.7.cloned.1.call-start = ((), (), s32[]{:S(2)}) async-start(), calls=%async_computation.3 | async-start | bytes 1024000 | tf_op jit(solution)/shard_map/reduce_scatter | solution.py:90
  18.3 7.6 %copy-start.10 = (s32[8]{0:T(128)S(1)}, s32[8]{0:T(128)}, u32[]{:S(2)}) copy-start(s32[8]{0:T(128)} %param.35) | copy-start | bytes 100
  18.3 7.6 %copy-start.11 = (f32[16]{0:T(128)S(1)}, f32[16]{0:T(128)}, u32[]{:S(2)}) copy-start(f32[16]{0:T(128)} %param.28) | copy-start | bytes 196
  18.3 7.7 %copy-start.5 = (bf16[4,1024]{1,0:T(4,128)(2,1)S(1)}, bf16[4,1024]{1,0:T(4,128)(2,1)}, u32[]{:S(2)}) copy-start(bf16[4,1024]{1,0:T(4,128)(2,1)} %param.25) | copy-start | bytes 24580
  18.4 7.7 %copy-start.6 = (bf16[4,1024]{1,0:T(4,128)(2,1)S(1)}, bf16[4,1024]{1,0:T(4,128)(2,1)}, u32[]{:S(2)}) copy-start(bf16[4,1024]{1,0:T(4,128)(2,1)} %param.26) | copy-start | bytes 24580
  18.4 8.0 %copy-start.7 = (bf16[1024]{0:T(1024)(128)(2,1)S(1)}, bf16[1024]{0:T(1024)(128)(2,1)}, u32[]{:S(2)}) copy-start(bf16[1024]{0:T(1024)(128)(2,1)} %param.30) | copy-start | bytes 6148
  18.4 8.9 %copy-start.4 = (bf16[8,7,1024]{2,0,1:T(8,128)(2,1)S(1)}, bf16[8,7,1024]{2,0,1:T(8,128)(2,1)}, u32[]{:S(2)}) copy-start(bf16[8,7,1024]{2,0,1:T(8,128)(2,1)} %param.34) | copy-start | bytes 344068
  25.8 130.0 %reduce-scatter.5.cloned.1.call-start = ((), (), s32[]{:S(2)}) async-start(), calls=%async_computation.2 | async-start | bytes 589824 | tf_op jit(solution)/shard_map/reduce_scatter | solution.py:137
  38.4 5.3 %copy-start.2 = (f32[8,16,64,128]{3,2,1,0:T(8,128)S(1)}, f32[8,16,64,128]{3,2,1,0:T(8,128)}, u32[]{:S(2)}) copy-start(f32[8,16,64,128]{3,2,1,0:T(8,128)} %gather_fusion) | copy-start | bytes 12582916
  38.6 12.4 %copy-start.8 = (f32[16]{0:T(128)S(1)}, f32[16]{0:T(128)}, u32[]{:S(2)}) copy-start(f32[16]{0:T(128)} %param.27) | copy-start | bytes 196
  73.7 6.2 %copy-start.3 = (f32[8,4,16,64,128]{4,1,3,2,0:T(4,128)}, f32[8,4,16,64,128]{4,1,3,2,0:T(4,128)S(1)}, u32[]{:S(2)}) copy-start(f32[8,4,16,64,128]{4,1,3,2,0:T(4,128)S(1)} %bitcast_add_fusion) | copy-start | bytes 50331652
  73.7 11.3 %copy-start.9 = (f32[16]{0:T(128)S(1)}, f32[16]{0:T(128)}, u32[]{:S(2)}) copy-start(f32[16]{0:T(128)} %param.29) | copy-start | bytes 196
  112.2 45.1 %copy-start.1 = (bf16[8,7,1024]{2,0,1:T(8,128)(2,1)S(1)}, bf16[8,7,1024]{2,0,1:T(8,128)(2,1)}, u32[]{:S(2)}) copy-start(bf16[8,7,1024]{2,0,1:T(8,128)(2,1)} %param.33) | copy-start | bytes 344068
Sparse Core Ops, SparseCore 0:
  25.9 23.7 reduce-scatter.6
  92.3 63.4 reduce-scatter.4
where the time goes:
time: 165 us; the launch traced here: 164 us
  local copies, waits for them, and re-layouts  46.8 us (28%)
  other arithmetic  38.2 us (23%)
  matrix products  32.2 us (20%)
  blocking collectives  30.2 us (18%)
  between operations  14.4 us (9%)
  waiting for transfers between devices  2.31 us (1%)
    unnamed x30, local copies, waits for them, and re-layouts  29.7 us
    psum x1, blocking collectives, local(): total_squares = lax.psum(square_sum, 'kv')  21.9 us
    concatenate x1, other arithmetic, local(): new_states = jnp.concatenate([first_state[:, None], states], axis=1)  20 us
    dot_general x1, matrix products, ssd_block(): jnp.einsum('strh,srhpn->sthpn', weights, outer_prod)  15.6 us
    select_n x2, other arithmetic, local(): jnp.take_along_axis(saved_states, accepted[:, None, None, None, None], ax...  11.7 us
    gather x1, local copies, waits for them, and re-layouts, local(): jnp.take_along_axis(saved_states, accepted[:, None, None, None, None], ax...  10.2 us
    psum x1, blocking collectives, local(): squares = lax.psum(jnp.sum(widened * widened, axis=1), 'tp')  8.36 us
    dot_general x1, matrix products, local(): jnp.dot(scaled, output_weight, preferred_element_type=jnp.float32)  5.75 us
  transfers between devices with their start and end apart: 2, of which 1 were waited for; matrix products, arithmetic and copies ran while one was open for 39% of the time, Pallas kernels for 0%

commit v1 on v0

--- a/solution.py
+++ b/solution.py
@@ -1,6 +1,10 @@
 import jax
 import jax.numpy as jnp
+import functools
+
 from jax import lax
+from jax.experimental import pallas as pl
+from jax.experimental.pallas import tpu as pltpu
 from jax.sharding import PartitionSpec as P
 
 D = 4096
@@ -54,7 +58,7 @@
     return (output, states)
 
 
-def local(
+def local_general(
     hidden,
     input_gain,
     x_weight,
@@ -139,6 +143,278 @@
     return (mixed, new_states, x_window, bc_window)
 
 
+NN = (((1,), (0,)), ((), ()))
+NT = (((1,), (1,)), ((), ()))
+TN = (((0,), (0,)), ((), ()))
+
+
+def dot(a, b, dims=NN, **kw):
+    return lax.dot_general(a, b, dims, preferred_element_type=jnp.float32, **kw)
+
+
+def silu(v):
+    return v / (1.0 + jnp.exp(-v))
+
+
+def softplus(v):
+    return jnp.maximum(v, 0.0) + jnp.log(1.0 + jnp.exp(-jnp.abs(v)))
+
+
+def mix_kernel(
+    features, channels, n_out,
+    acc_smem, acc_ref, proj_ref, xh_ref, bch_ref, xk_ref, bck_ref, par_ref, gain_ref,
+    saved_ref, w_ref,
+    part_ref, xw_ref, bcw_ref, xdt_ref, b_ref, a_ref,
+    s0_buf, w_buf, s0_sem, w_sem,
+):
+    seqs = acc_smem.shape[0]
+    props = proj_ref.shape[0] // seqs
+    rows = seqs * props
+    inner = xh_ref.shape[2]
+    bcw = bch_ref.shape[2]
+    heads, size, state = s0_buf.shape[1:]
+    groups = bcw // (2 * state)
+    per = heads // groups
+    span = per * size
+
+    def s0_copy(s):
+        return pltpu.make_async_copy(
+            saved_ref.at[s, acc_smem[s]], s0_buf.at[s], s0_sem.at[s])
+
+    for s in range(seqs):
+        s0_copy(s).start()
+    block = w_ref.shape[1] // n_out
+    w_copies = [
+        pltpu.make_async_copy(
+            w_ref.at[:, pl.ds(i * block, block)], w_buf.at[i], w_sem.at[i])
+        for i in range(n_out)
+    ]
+    for copy in w_copies:
+        copy.start()
+
+    ri = lax.broadcasted_iota(jnp.int32, (rows, rows), 0)
+    ci = lax.broadcasted_iota(jnp.int32, (rows, rows), 1)
+    to_steps = ((ri % seqs) * props + ri // seqs == ci).astype(jnp.float32).astype(jnp.bfloat16)
+    back = ((ci % seqs) * props + ci // seqs == ri).astype(jnp.float32).astype(jnp.bfloat16)
+
+    dt_at = 2 * inner + bcw
+    last = proj_ref.shape[1]
+    squares = proj_ref[:, last - 128 :].astype(jnp.float32)[:, 127:128]
+    scale = lax.rsqrt(squares / features + EPSILON)
+
+    def fresh(lo, hi):
+        v = (proj_ref[:, lo:hi].astype(jnp.float32) * scale).astype(jnp.bfloat16)
+        return dot(to_steps, v)
+
+    def step(v, t):
+        return v[t * seqs : (t + 1) * seqs]
+
+    acc = acc_ref[...]
+
+    def window(hist_ref, rows_fresh, out_ref):
+        kept = hist_ref.shape[0] - props
+        hist = [hist_ref[m].astype(jnp.float32) for m in range(hist_ref.shape[0])]
+        win = []
+        for k in range(kept):
+            v = hist[k]
+            for j in range(1, props + 1):
+                v = jnp.where(acc == j, hist[j + k], v)
+            win.append(v)
+        win += [step(rows_fresh, t) for t in range(props)]
+        for m, v in enumerate(win):
+            out_ref[m] = v.astype(jnp.bfloat16)
+        return win
+
+    def conv(win, kernel_ref):
+        taps = [kernel_ref[j : j + 1].astype(jnp.float32) for j in range(kernel_ref.shape[0])]
+        out = []
+        for t in range(props):
+            v = win[t] * taps[0]
+            for j in range(1, len(taps)):
+                v = v + win[t + j] * taps[j]
+            out.append(silu(v))
+        return out
+
+    bc = conv(window(bch_ref, fresh(2 * inner, dt_at), bcw_ref), bck_ref)
+    b_all = jnp.concatenate(
+        [jnp.concatenate([v[:, 2 * g * state : (2 * g + 1) * state] for g in range(groups)], axis=1) for v in bc], axis=0)
+    c_all = jnp.concatenate(
+        [jnp.concatenate([v[:, (2 * g + 1) * state : (2 * g + 2) * state] for g in range(groups)], axis=1) for v in bc], axis=0)
+    b_ref[...] = b_all.astype(jnp.bfloat16)
+    c_low = c_all.astype(jnp.bfloat16)
+    xc = conv(window(xh_ref, fresh(0, inner), xw_ref), xk_ref)
+
+    dt_raw = fresh(dt_at, last)
+    eh = lax.broadcasted_iota(jnp.int32, (128, inner), 0)
+    ec = lax.broadcasted_iota(jnp.int32, (128, inner), 1)
+    expand = (eh == ec // size).astype(jnp.float32)
+    par = par_ref[...]
+    wide = dot(par, expand, precision=lax.Precision.HIGHEST)
+    dtw = dot(dt_raw.astype(jnp.bfloat16), expand.astype(jnp.bfloat16))
+    lane = lax.broadcasted_iota(jnp.int32, (rows, 128), 1)
+    raw = jnp.where(lane < heads, dt_raw, 0.0)
+    a_ref[...] = jnp.exp(-jnp.exp(par[1:2]) * softplus(raw + par[0:1]))
+    bias, rate, skip = wide[0:1], jnp.exp(wide[1:2]), wide[2:3]
+    sizes = [softplus(step(dtw, t) + bias) for t in range(props)]
+    xdt = [xc[t] * sizes[t] for t in range(props)]
+    xdt_ref[...] = jnp.concatenate(xdt, axis=0).astype(jnp.bfloat16)
+
+    row = lax.broadcasted_iota(jnp.int32, (rows, span), 0)
+    carried = [jnp.zeros((rows, span), jnp.float32) for _ in range(groups)]
+    for s in range(seqs):
+        s0_copy(s).wait()
+        for g in range(groups):
+            s0 = s0_buf[s, g * per : (g + 1) * per].reshape(span, state).astype(jnp.bfloat16)
+            got = dot(c_low[:, g * state : (g + 1) * state], s0, NT)
+            carried[g] = jnp.where(row % seqs == s, got, carried[g])
+    carried = jnp.concatenate(carried, axis=1)
+
+    decays = [-rate * v for v in sizes]
+    gated, sums = [], []
+    zs = fresh(inner, 2 * inner)
+    gain = gain_ref[...].astype(jnp.float32)
+    for t in range(props):
+        total = decays[t]
+        out = skip * xc[t]
+        ct = step(c_all, t)
+        for r in range(t, -1, -1):
+            br = step(b_all, r)
+            prod = ct * br
+            pair = jnp.concatenate(
+                [jnp.broadcast_to(
+                    jnp.sum(prod[:, g * state : (g + 1) * state], axis=1, keepdims=True),
+                    (seqs, span)) for g in range(groups)], axis=1)
+            if r == t:
+                out = out + pair * xdt[r]
+            else:
+                out = out + jnp.exp(total) * pair * xdt[r]
+                total = total + decays[r]
+        out = out + jnp.exp(total) * step(carried, t)
+        v = out * silu(step(zs, t))
+        gated.append((v * gain).astype(jnp.bfloat16))
+        sums.append(jnp.broadcast_to(jnp.sum(v * v, axis=1, keepdims=True), (seqs, 128)))
+    scaled = dot(back, jnp.concatenate(gated, axis=0)).astype(jnp.bfloat16)
+    sums = jnp.concatenate(sums, axis=0)
+    high = sums.astype(jnp.bfloat16)
+    low = (sums - high.astype(jnp.float32)).astype(jnp.bfloat16)
+    sums = dot(back, high) + dot(back, low)
+    for i in range(n_out):
+        w_copies[i].wait()
+        part_ref[i, :, :block] = dot(scaled, w_buf[i]).astype(part_ref.dtype)
+        part_ref[i, :, block:] = sums.astype(part_ref.dtype)
+
+
+def state_kernel(acc_smem, a_smem, xdt_ref, b_ref, s0_ref, out_ref):
+    s = pl.program_id(0)
+    seqs = acc_smem.shape[0]
+    rows = xdt_ref.shape[0]
+    props = rows // seqs
+    heads, size, state = s0_ref.shape[2:]
+    groups = b_ref.shape[1] // state
+    per = heads // groups
+    row = lax.broadcasted_iota(jnp.int32, (rows, state), 0)
+    first = s0_ref[0, 0]
+    out_ref[0, 0] = first
+    for g in range(groups):
+        b = b_ref[:, g * state : (g + 1) * state].astype(jnp.float32)
+        masked = jnp.concatenate(
+            [jnp.where(row == t * seqs + s, b, 0.0) for t in range(props)], axis=1).astype(jnp.bfloat16)
+        x = xdt_ref[:, g * per * size : (g + 1) * per * size]
+        outer = dot(x, masked, TN)
+        for h in range(per):
+            head = g * per + h
+            now = first[head]
+            for t in range(props):
+                now = a_smem[t * seqs + s, head] * now + outer[
+                    h * size : (h + 1) * size, t * state : (t + 1) * state]
+                out_ref[0, t + 1, head] = now
+
+
+def local(
+    hidden, input_gain, x_weight, z_weight, bc_weight, dt_weight, x_kernel, bc_kernel,
+    dt_bias, decay_log, skip_scale, output_gain, output_weight, saved_states,
+    x_history, bc_history, accepted,
+):
+    heads = dt_bias.shape[0]
+    seqs, slots, _, size, state = saved_states.shape
+    hist = x_history.shape[1]
+    inner, bcw = x_weight.shape[1], bc_weight.shape[1]
+    n_kv, n_tp = lax.axis_size("kv"), lax.axis_size("tp")
+    rows = hidden.shape[0] // n_tp
+    n_col = output_weight.shape[1]
+    widened = hidden.astype(jnp.float32)
+    squares = jnp.sum(widened * widened, axis=1, keepdims=True)
+    entry = (widened * input_gain.astype(jnp.float32)).astype(jnp.bfloat16)
+    weights = jnp.concatenate([x_weight, z_weight, bc_weight, dt_weight], axis=1)
+    product = jnp.dot(entry, weights, preferred_element_type=jnp.float32).astype(jnp.bfloat16)
+    fill = jnp.broadcast_to(squares.astype(jnp.bfloat16), (hidden.shape[0], 128 - heads))
+    projected = lax.psum_scatter(
+        jnp.concatenate([product, fill], axis=1), "tp", scatter_dimension=0, tiled=True)
+
+    params = jnp.pad(jnp.stack([dt_bias, decay_log, skip_scale]), ((0, 5), (0, 128 - heads)))
+    vmem = pl.BlockSpec(memory_space=pltpu.VMEM)
+    anym = pl.BlockSpec(memory_space=pl.ANY)
+    smem = pl.BlockSpec(memory_space=pltpu.SMEM)
+    block = n_col // n_kv
+    part, xw, bcw_out, xdt, b, a = pl.pallas_call(
+        functools.partial(mix_kernel, hidden.shape[1] * n_tp, inner * n_kv, n_kv),
+        out_shape=(
+            jax.ShapeDtypeStruct((n_kv, rows, block + 128), jnp.bfloat16),
+            jax.ShapeDtypeStruct((hist, seqs, inner), jnp.bfloat16),
+            jax.ShapeDtypeStruct((hist, seqs, bcw), jnp.bfloat16),
+            jax.ShapeDtypeStruct((rows, inner), jnp.bfloat16),
+            jax.ShapeDtypeStruct((rows, bcw // 2), jnp.bfloat16),
+            jax.ShapeDtypeStruct((rows, 128), jnp.float32),
+        ),
+        in_specs=[smem] + [vmem] * 8 + [anym] * 2,
+        out_specs=[vmem] * 6,
+        scratch_shapes=[
+            pltpu.VMEM((seqs, heads, size, state), jnp.float32),
+            pltpu.VMEM((n_kv, inner, block), jnp.bfloat16),
+            pltpu.SemaphoreType.DMA((seqs,)),
+            pltpu.SemaphoreType.DMA((n_kv,)),
+        ],
+        compiler_params=pltpu.CompilerParams(vmem_limit_bytes=40 << 20),
+        cost_estimate=pl.CostEstimate(
+            flops=2 * rows * inner * n_col, bytes_accessed=14 << 20, transcendentals=0),
+        name="mix",
+    )(
+        accepted, accepted[:, None], projected,
+        x_history.transpose(1, 0, 2), bc_history.transpose(1, 0, 2),
+        x_kernel, bc_kernel, params, output_gain[None, :], saved_states, output_weight,
+    )
+    summed = lax.psum_scatter(part, "kv", scatter_dimension=0, tiled=True)[0]
+
+    new_states = pl.pallas_call(
+        state_kernel,
+        out_shape=jax.ShapeDtypeStruct(saved_states.shape, jnp.float32),
+        grid_spec=pltpu.PrefetchScalarGridSpec(
+            num_scalar_prefetch=1,
+            grid=(seqs,),
+            in_specs=[
+                smem,
+                pl.BlockSpec((rows, inner), lambda s, acc: (0, 0)),
+                pl.BlockSpec((rows, bcw // 2), lambda s, acc: (0, 0)),
+                pl.BlockSpec((1, 1, heads, size, state), lambda s, acc: (s, acc[s], 0, 0, 0)),
+            ],
+            out_specs=pl.BlockSpec((1, slots, heads, size, state), lambda s, acc: (s, 0, 0, 0, 0)),
+        ),
+        compiler_params=pltpu.CompilerParams(vmem_limit_bytes=24 << 20),
+        cost_estimate=pl.CostEstimate(
+            flops=2 * saved_states.size, bytes_accessed=6 * saved_states.size, transcendentals=0),
+        name="states",
+    )(accepted, a, xdt, b, saved_states)
+
+    norm = lax.rsqrt(summed[:, block : block + 1].astype(jnp.float32) / (inner * n_kv) + EPSILON)
+    mixed = (norm * summed[:, :block].astype(jnp.float32)).astype(jnp.bfloat16)
+    return (mixed, new_states, xw.transpose(1, 0, 2), bcw_out.transpose(1, 0, 2))
+
+
+def fits(mesh):
+    inner = INNER // mesh.shape["kv"]
+    return inner % 1024 == 0 and mesh.shape["kv"] > 1
+
+
 def solution(mesh):
     in_specs = (
         P(None, "tp"),
@@ -165,4 +441,5 @@
         P("tp", None, "kv"),
         P("tp", None, "kv"),
     )
-    return jax.shard_map(local, mesh=mesh, in_specs=in_specs, out_specs=out_specs, check_vma=False)
+    body = local if fits(mesh) else local_general
+    return jax.shard_map(body, mesh=mesh, in_specs=in_specs, out_specs=out_specs, check_vma=False)

time: 165 us -> 128 us (0.78)
  waiting for transfers between devices: 2.31 us -> 71.4 us
  local copies, waits for them, and re-layouts: 46.8 us -> 13.5 us
  other arithmetic: 38.2 us -> 5.03 us
  blocking collectives: 30.2 us -> 0 us
  matrix products: 32.2 us -> 5.68 us
  Pallas kernels: 0 us -> 17.5 us
    reduce_scatter x2, waiting for transfers between devices: 2.28 us -> 71.4 us  [the longest x1 45.2 us: local(): summed = lax.psum_scatter(part, 'kv', scatter_dimension=0, tiled=True)[0]]
    psum x2 -> x0, blocking collectives: 30.2 us -> none  [the longest x1 21.9 us: local(): total_squares = lax.psum(square_sum, 'kv')]
    dot_general x4 -> x1, matrix products: 32.2 us -> 5.68 us  [local(): jnp.dot(entry, weights, preferred_element_type=jnp.float32)]
    concatenate x2 -> x1, other arithmetic: 20.2 us -> 0.99 us  [local(): jnp.concatenate([product, fill], axis=1)]
    pallas_call x0 -> x2, Pallas kernels: none -> 17.5 us  [the longest x1 10.1 us: local(): pl.pallas_call(state_kernel, out_shape=jax.ShapeDtypeStruct(saved_states....]
    unnamed x30 -> x25, local copies, waits for them, and re-layouts: 29.7 us -> 12.2 us
    gather x7 -> x0, local copies, waits for them, and re-layouts: 12.2 us -> none  [the longest x1 10.2 us: local(): jnp.take_along_axis(saved_states, accepted[:, None, None, None, None], ax...]
    select_n x3 -> x0, other arithmetic: 11.8 us -> none  [the longest x2 11.7 us: local(): jnp.take_along_axis(saved_states, accepted[:, None, None, None, None], ax...]
  transfers between devices with their start and end apart: 2 -> 2, of which waited for: 1 -> 2; matrix products, arithmetic and copies ran while one was open for 39% -> 0% of each run, Pallas kernels for 0% -> 8%
where the time goes in v1:
time: 128 us; the launch traced here: 127 us
  waiting for transfers between devices  71.4 us (56%)
  Pallas kernels  17.5 us (14%)
  between operations  14.2 us (11%)
  local copies, waits for them, and re-layouts  13.5 us (11%)
  matrix products  5.68 us (4%)
  other arithmetic  5.03 us (4%)
    reduce_scatter x1, waiting for transfers between devices, local(): summed = lax.psum_scatter(part, 'kv', scatter_dimension=0, tiled=True)[0]  45.2 us
    reduce_scatter x1, waiting for transfers between devices, local(): lax.psum_scatter(jnp.concatenate([product, fill], axis=1), 'tp', scatter_...  26.1 us
    unnamed x25, local copies, waits for them, and re-layouts  12.2 us
    pallas_call x1, Pallas kernels, local(): pl.pallas_call(state_kernel, out_shape=jax.ShapeDtypeStruct(saved_states....  10.1 us
    pallas_call x1, Pallas kernels, local(): pl.pallas_call(functools.partial(mix_kernel, hidden.shape[1] * n_tp, inne...  7.44 us
    dot_general x1, matrix products, local(): jnp.dot(entry, weights, preferred_element_type=jnp.float32)  5.68 us
  transfers between devices with their start and end apart: 2, of which 2 were waited for; matrix products, arithmetic and copies ran while one was open for 0% of the time, Pallas kernels for 8%

profile of v1, /device:TPU:0, one launch (start us, length us, event | category | flops | bytes accessed | tf_op | source)
XLA Modules:
  0.0 127.4 jit_solution(2641442610720500199)
XLA Ops:
  7.2 0.0 reduce-scatter.3.cloned.1.call-start
  7.2 1.1 fusion.12
  8.3 0.7 convert_element_type.32
  9.0 0.9 copy.27
  9.9 0.0 copy-start.8
  9.9 0.0 copy-start.7
  9.9 0.0 copy-start.9
  9.9 0.0 copy-start.10
  10.0 0.0 copy-start.11
  10.0 0.0 copy-start.3
  10.0 0.0 copy-start.4
  10.0 0.0 copy-start.5
  10.0 0.0 copy-start.6
  10.0 5.7 %fusion.8 = bf16[128,3088]{0,1:T(8,128)(2,1)S(1)} fusion(bf16[1024,16]{1,0:T(8,128)(2,1)S(1)} %copy.27, bf16[1024,1024]{1,0:T(8,128)(2,1)} %param.21, bf16[1024,1024]{1,0:T(8,128)(2,1)} %param.20, bf16[1024,1024]{1,0:T(8,128)(2,1)} %param.19, bf16[128,1024]{1,0:T(8,128)(2,1)} %param.17, f32[1024]{0:T(1024)S(1)} %convert_element_type.32), kind=kOutput, calls=%fused_computation.8 | convolution fusion | flops 835586048 | bytes 7380992 | tf_op jit(solution)/shard_map/dot_general | solution.py:349
  15.7 1.1 copy.28
  16.8 0.1 broadcast_in_dim.14
  16.9 1.0 pad_maximum_fusion
  17.9 0.0 reduce-scatter.3.cloned.1.call-update
  17.9 0.0 reduce-scatter.5.cloned.1.call-start
  17.9 0.0 copy-done.8
  18.0 0.0 copy-done.7
  18.0 0.1 copy.29.acc_ref
  18.0 0.0 copy-done.9
  18.0 0.0 copy-done.10
  18.1 0.0 copy-done.11
  18.1 26.1 %reduce-scatter.3.cloned.1.call-done.proj_ref = bf16[32,3200]{1,0:T(8,128)(2,1)} async-done(((bf16[128,3200]{1,0:T(8,128)(2,1)}), bf16[32,3200]{1,0:T(8,128)(2,1)}) %reduce-scatter.3.cloned.1.call-update) | async-done | bytes 204816 | tf_op jit(solution)/shard_map/reduce_scatter | solution.py:351
  44.2 0.0 copy-done.3
  44.2 0.0 copy-done.4
  44.2 0.0 copy-done.5
  44.2 0.0 copy-done.6
  44.2 0.0 copy-start.1
  44.2 3.4 %copy-done.1 = bf16[1024,4096]{1,0:T(8,128)(2,1)S(1)} copy-done((bf16[1024,4096]{1,0:T(8,128)(2,1)S(1)}, bf16[1024,4096]{1,0:T(8,128)(2,1)}, u32[]{:S(2)}) %copy-start.1) | copy-done | bytes 8388632
  47.6 0.0 copy-start.2
  47.6 0.9 copy-done.2
  48.5 7.4 %mix.1 = (bf16[8,32,640]{2,1,0:T(8,128)(2,1)}, bf16[7,8,1024]{2,1,0:T(8,128)(2,1)}, bf16[7,8,1024]{2,1,0:T(8,128)(2,1)}, bf16[32,1024]{1,0:T(8,128)(2,1)S(1)}, b...) custom-call(s32[8]{0:T(128)S(1)} %copy-done.7, s32[8,1]{1,0:T(8,128)S(1)} %copy.29.acc_ref, ...), custom_call_target="tpu_custom_call" | custom-call | flops 268435456 | bytes 14680064 | tf_op jit(solution)/shard_map/mix/pallas_call | solution.py:359
  56.0 0.0 reduce-scatter.5.cloned.1.call-update
  56.0 0.0 copy-start
  56.0 7.0 %copy-done = f32[8,5,16,64,128]{4,3,2,1,0:T(8,128)S(1)} copy-done((f32[8,5,16,64,128]{4,3,2,1,0:T(8,128)S(1)}, f32[8,5,16,64,128]{4,3,2,1,0:T(8,128)}, u32[]{:S(2)}) %copy-start) | copy-done | bytes 20971544
  63.0 10.1 %states.1 = f32[8,5,16,64,128]{4,3,2,1,0:T(8,128)} custom-call(s32[8]{0:T(128)S(1)} %copy-done.7, f32[32,128]{1,0:T(8,128)S(1)} %get-tuple-element.11.a_smem, bf16[32,1024]{1,0:T(8,128)(2,1)S(1)} %get-tuple-element.12.xdt_ref, bf16[32,512]{1,0:T(8,128)(2,1)S(1)} %get-tuple-element.13.b_ref, f32[8,5,16,64,128]{4,3,2,1,0:T(8,128)S(1)} %copy-done), custom_call_target="tpu_custom_call" | custom-call | flops 10485760 | bytes 31457280 | tf_op jit(solution)/shard_map/states/pallas_call | solution.py:388
  73.0 45.2 %reduce-scatter.5.cloned.1.call-done = bf16[1,32,640]{2,1,0:T(8,128)(2,1)} async-done(((bf16[8,32,640]{2,1,0:T(8,128)(2,1)}), bf16[1,32,640]{2,1,0:T(8,128)(2,1)}) %reduce-scatter.5.cloned.1.call-update) | async-done | bytes 40976 | tf_op jit(solution)/shard_map/reduce_scatter | solution.py:386
  118.3 0.8 rsqrt_reduce_fusion
  119.1 1.5 %multiply_convert_fusion = bf16[32,512]{1,0:T(8,128)(2,1)} fusion(bf16[32,640]{1,0:T(8,128)(2,1)} %bitcast.13, f32[32]{0:T(128)S(1)} %rsqrt_reduce_fusion), kind=kLoop, calls=%fused_computation.15 | loop fusion | flops 49152 | bytes 65664 | tf_op jit(solution)/shard_map/convert_element_type | solution.py:409
  (2 shorter events, 0.0 us)
Async XLA Ops:
  7.2 37.0 %reduce-scatter.3.cloned.1.call-start = ((), (), s32[]{:S(2)}) async-start(), calls=%async_computation.2 | async-start | bytes 1024000 | tf_op jit(solution)/shard_map/reduce_scatter | solution.py:351
  9.9 8.0 %copy-start.8 = (bf16[1024]{0:T(1024)(128)(2,1)S(1)}, bf16[1024]{0:T(1024)(128)(2,1)}, u32[]{:S(2)}) copy-start(bf16[1024]{0:T(1024)(128)(2,1)} %param.28) | copy-start | bytes 6148
  9.9 8.0 %copy-start.7 = (s32[8]{0:T(128)S(1)}, s32[8]{0:T(128)}, u32[]{:S(2)}) copy-start(s32[8]{0:T(128)} %acc_smem.3) | copy-start | bytes 100
  9.9 8.1 %copy-start.9 = (f32[16]{0:T(128)S(1)}, f32[16]{0:T(128)}, u32[]{:S(2)}) copy-start(f32[16]{0:T(128)} %param.27) | copy-start | bytes 196
  9.9 8.1 %copy-start.10 = (f32[16]{0:T(128)S(1)}, f32[16]{0:T(128)}, u32[]{:S(2)}) copy-start(f32[16]{0:T(128)} %param.26) | copy-start | bytes 196
  10.0 8.1 %copy-start.11 = (f32[16]{0:T(128)S(1)}, f32[16]{0:T(128)}, u32[]{:S(2)}) copy-start(f32[16]{0:T(128)} %param.25) | copy-start | bytes 196
  10.0 34.2 %copy-start.3 = (bf16[8,7,1024]{2,0,1:T(8,128)(2,1)S(1)}, bf16[8,7,1024]{2,0,1:T(8,128)(2,1)}, u32[]{:S(2)}) copy-start(bf16[8,7,1024]{2,0,1:T(8,128)(2,1)} %param.31) | copy-start | bytes 344068
  10.0 34.2 %copy-start.4 = (bf16[8,7,1024]{2,0,1:T(8,128)(2,1)S(1)}, bf16[8,7,1024]{2,0,1:T(8,128)(2,1)}, u32[]{:S(2)}) copy-start(bf16[8,7,1024]{2,0,1:T(8,128)(2,1)} %param.32) | copy-start | bytes 344068
  10.0 34.2 %copy-start.5 = (bf16[4,1024]{1,0:T(4,128)(2,1)S(1)}, bf16[4,1024]{1,0:T(4,128)(2,1)}, u32[]{:S(2)}) copy-start(bf16[4,1024]{1,0:T(4,128)(2,1)} %xk_ref.1) | copy-start | bytes 24580
  10.0 34.2 %copy-start.6 = (bf16[4,1024]{1,0:T(4,128)(2,1)S(1)}, bf16[4,1024]{1,0:T(4,128)(2,1)}, u32[]{:S(2)}) copy-start(bf16[4,1024]{1,0:T(4,128)(2,1)} %bck_ref.1) | copy-start | bytes 24580
  17.9 100.4 %reduce-scatter.5.cloned.1.call-start = ((), (), s32[]{:S(2)}) async-start(), calls=%async_computation.3 | async-start | bytes 368640 | tf_op jit(solution)/shard_map/reduce_scatter | solution.py:386
  44.2 3.4 %copy-start.1 = (bf16[1024,4096]{1,0:T(8,128)(2,1)S(1)}, bf16[1024,4096]{1,0:T(8,128)(2,1)}, u32[]{:S(2)}) copy-start(bf16[1024,4096]{1,0:T(8,128)(2,1)} %w_ref.1) | copy-start | bytes 25165828
  47.6 0.9 copy-start.2
  56.0 7.0 %copy-start = (f32[8,5,16,64,128]{4,3,2,1,0:T(8,128)S(1)}, f32[8,5,16,64,128]{4,3,2,1,0:T(8,128)}, u32[]{:S(2)}) copy-start(f32[8,5,16,64,128]{4,3,2,1,0:T(8,128)} %s0_ref.1) | copy-start | bytes 62914564
Sparse Core Ops, SparseCore 0:
  18.0 26.1 reduce-scatter.2
  56.1 62.1 reduce-scatter.4

commit v2 on v1

--- a/solution.py
+++ b/solution.py
@@ -162,7 +162,7 @@
 
 def mix_kernel(
     features, channels, n_out,
-    acc_smem, acc_ref, proj_ref, xh_ref, bch_ref, xk_ref, bck_ref, par_ref, gain_ref,
+    acc_smem, bias_smem, decay_smem, skip_smem, proj_ref, xh_ref, bch_ref, xk_ref, bck_ref, gain_ref,
     saved_ref, w_ref,
     part_ref, xw_ref, bcw_ref, xdt_ref, b_ref, a_ref,
     s0_buf, w_buf, s0_sem, w_sem,
@@ -209,7 +209,10 @@
     def step(v, t):
         return v[t * seqs : (t + 1) * seqs]
 
-    acc = acc_ref[...]
+    seq_at = lax.broadcasted_iota(jnp.int32, (seqs, inner), 0)
+    acc = jnp.zeros((seqs, inner), jnp.int32)
+    for s in range(seqs):
+        acc = jnp.where(seq_at == s, acc_smem[s], acc)
 
     def window(hist_ref, rows_fresh, out_ref):
         kept = hist_ref.shape[0] - props
@@ -218,7 +221,7 @@
         for k in range(kept):
             v = hist[k]
             for j in range(1, props + 1):
-                v = jnp.where(acc == j, hist[j + k], v)
+                v = jnp.where(acc[:, :1] == j, hist[j + k], v)
             win.append(v)
         win += [step(rows_fresh, t) for t in range(props)]
         for m, v in enumerate(win):
@@ -248,7 +251,12 @@
     eh = lax.broadcasted_iota(jnp.int32, (128, inner), 0)
     ec = lax.broadcasted_iota(jnp.int32, (128, inner), 1)
     expand = (eh == ec // size).astype(jnp.float32)
-    par = par_ref[...]
+    lane_at = lax.broadcasted_iota(jnp.int32, (8, 128), 1)
+    row_at = lax.broadcasted_iota(jnp.int32, (8, 128), 0)
+    par = jnp.zeros((8, 128), jnp.float32)
+    for i, smem in enumerate((bias_smem, decay_smem, skip_smem)):
+        for h in range(heads):
+            par = jnp.where((row_at == i) & (lane_at == h), smem[h], par)
     wide = dot(par, expand, precision=lax.Precision.HIGHEST)
     dtw = dot(dt_raw.astype(jnp.bfloat16), expand.astype(jnp.bfloat16))
     lane = lax.broadcasted_iota(jnp.int32, (rows, 128), 1)
@@ -272,7 +280,7 @@
     decays = [-rate * v for v in sizes]
     gated, sums = [], []
     zs = fresh(inner, 2 * inner)
-    gain = gain_ref[...].astype(jnp.float32)
+    gain = gain_ref[...].astype(jnp.float32).reshape(1, inner)
     for t in range(props):
         total = decays[t]
         out = skip * xc[t]
@@ -330,6 +338,64 @@
                 out_ref[0, t + 1, head] = now
 
 
+def exchange(axis, blocks_ref, slots, send_sems, recv_sems):
+    count = blocks_ref.shape[0]
+    me = lax.axis_index(axis)
+    barrier = pltpu.get_barrier_semaphore()
+    for d in range(1, count):
+        pl.semaphore_signal(
+            barrier, inc=1, device_id={axis: lax.rem(me + d, count)}, device_id_type=pl.DeviceIdType.MESH)
+    pl.semaphore_wait(barrier, count - 1)
+    copies = []
+    for d in range(1, count):
+        peer = lax.rem(me + d, count)
+        copies.append(pltpu.make_async_remote_copy(
+            src_ref=blocks_ref.at[peer],
+            dst_ref=slots.at[d - 1],
+            send_sem=send_sems.at[d - 1],
+            recv_sem=recv_sems.at[d - 1],
+            device_id={axis: peer},
+            device_id_type=pl.DeviceIdType.MESH,
+        ))
+    for copy in copies:
+        copy.start()
+    total = blocks_ref[me].astype(jnp.float32)
+    for d, copy in enumerate(copies):
+        copy.wait_recv()
+        total = total + slots[d].astype(jnp.float32)
+    for copy in copies:
+        copy.wait_send()
+    return total
+
+
+def entry_kernel(blocks_ref, out_ref, *scratch):
+    out_ref[...] = exchange("tp", blocks_ref, *scratch)
+
+
+def exit_kernel(channels, blocks_ref, out_ref, *scratch):
+    total = exchange("kv", blocks_ref, *scratch)
+    width = out_ref.shape[1]
+    norm = lax.rsqrt(total[:, width : width + 1] / channels + EPSILON)
+    out_ref[...] = (norm * total[:, :width]).astype(out_ref.dtype)
+
+
+def exchange_call(body, name, number, blocks, out_shape):
+    count = blocks.shape[0]
+    return pl.pallas_call(
+        body,
+        out_shape=out_shape,
+        in_specs=[pl.BlockSpec(memory_space=pltpu.VMEM)],
+        out_specs=pl.BlockSpec(memory_space=pltpu.VMEM),
+        scratch_shapes=[
+            pltpu.VMEM((count - 1,) + blocks.shape[1:], blocks.dtype),
+            pltpu.SemaphoreType.DMA((count - 1,)),
+            pltpu.SemaphoreType.DMA((count - 1,)),
+        ],
+        compiler_params=pltpu.CompilerParams(collective_id=number, has_side_effects=True),
+        name=name,
+    )(blocks)
+
+
 def local(
     hidden, input_gain, x_weight, z_weight, bc_weight, dt_weight, x_kernel, bc_kernel,
     dt_bias, decay_log, skip_scale, output_gain, output_weight, saved_states,
@@ -348,10 +414,11 @@
     weights = jnp.concatenate([x_weight, z_weight, bc_weight, dt_weight], axis=1)
     product = jnp.dot(entry, weights, preferred_element_type=jnp.float32).astype(jnp.bfloat16)
     fill = jnp.broadcast_to(squares.astype(jnp.bfloat16), (hidden.shape[0], 128 - heads))
-    projected = lax.psum_scatter(
-        jnp.concatenate([product, fill], axis=1), "tp", scatter_dimension=0, tiled=True)
-
-    params = jnp.pad(jnp.stack([dt_bias, decay_log, skip_scale]), ((0, 5), (0, 128 - heads)))
+    projected = exchange_call(
+        entry_kernel, "entry_exchange", 0,
+        jnp.concatenate([product, fill], axis=1).reshape(n_tp, rows, -1),
+        jax.ShapeDtypeStruct((rows, product.shape[1] + 128 - heads), jnp.float32))
+
     vmem = pl.BlockSpec(memory_space=pltpu.VMEM)
     anym = pl.BlockSpec(memory_space=pl.ANY)
     smem = pl.BlockSpec(memory_space=pltpu.SMEM)
@@ -366,7 +433,7 @@
             jax.ShapeDtypeStruct((rows, bcw // 2), jnp.bfloat16),
             jax.ShapeDtypeStruct((rows, 128), jnp.float32),
         ),
-        in_specs=[smem] + [vmem] * 8 + [anym] * 2,
+        in_specs=[smem] * 4 + [vmem] * 6 + [anym] * 2,
         out_specs=[vmem] * 6,
         scratch_shapes=[
             pltpu.VMEM((seqs, heads, size, state), jnp.float32),
@@ -374,16 +441,18 @@
             pltpu.SemaphoreType.DMA((seqs,)),
             pltpu.SemaphoreType.DMA((n_kv,)),
         ],
-        compiler_params=pltpu.CompilerParams(vmem_limit_bytes=40 << 20),
+        compiler_params=pltpu.CompilerParams(vmem_limit_bytes=60 << 20),
         cost_estimate=pl.CostEstimate(
             flops=2 * rows * inner * n_col, bytes_accessed=14 << 20, transcendentals=0),
         name="mix",
     )(
-        accepted, accepted[:, None], projected,
+        accepted, dt_bias, decay_log, skip_scale, projected,
         x_history.transpose(1, 0, 2), bc_history.transpose(1, 0, 2),
-        x_kernel, bc_kernel, params, output_gain[None, :], saved_states, output_weight,
-    )
-    summed = lax.psum_scatter(part, "kv", scatter_dimension=0, tiled=True)[0]
+        x_kernel, bc_kernel, output_gain, saved_states, output_weight,
+    )
+    mixed = exchange_call(
+        functools.partial(exit_kernel, inner * n_kv), "exit_exchange", 1, part,
+        jax.ShapeDtypeStruct((rows, block), jnp.bfloat16))
 
     new_states = pl.pallas_call(
         state_kernel,
@@ -399,14 +468,12 @@
             ],
             out_specs=pl.BlockSpec((1, slots, heads, size, state), lambda s, acc: (s, 0, 0, 0, 0)),
         ),
-        compiler_params=pltpu.CompilerParams(vmem_limit_bytes=24 << 20),
+        compiler_params=pltpu.CompilerParams(vmem_limit_bytes=60 << 20),
         cost_estimate=pl.CostEstimate(
             flops=2 * saved_states.size, bytes_accessed=6 * saved_states.size, transcendentals=0),
         name="states",
     )(accepted, a, xdt, b, saved_states)
 
-    norm = lax.rsqrt(summed[:, block : block + 1].astype(jnp.float32) / (inner * n_kv) + EPSILON)
-    mixed = (norm * summed[:, :block].astype(jnp.float32)).astype(jnp.bfloat16)
     return (mixed, new_states, xw.transpose(1, 0, 2), bcw_out.transpose(1, 0, 2))
 
 

time: 128 us -> 59.8 us (0.47)
  waiting for transfers between devices: 71.4 us -> 0 us
  Pallas kernels: 17.5 us -> 47.8 us
  between operations: 14.2 us -> 0.68 us
  local copies, waits for them, and re-layouts: 13.5 us -> 3.01 us
  other arithmetic: 5.03 us -> 1.83 us
    reduce_scatter x2 -> x0, waiting for transfers between devices: 71.4 us -> none  [the longest x1 45.2 us: local(): summed = lax.psum_scatter(part, 'kv', scatter_dimension=0, tiled=True)[0]]
    pallas_call x0 -> x2, Pallas kernels: none -> 27.1 us  [exchange_call(): pl.pallas_call(body, out_shape=out_shape, in_specs=[pl.BlockSpec(memory_s...]
    unnamed x25 -> x4, local copies, waits for them, and re-layouts: 12.2 us -> 1.54 us
    pallas_call x1, Pallas kernels: 7.44 us -> 9.18 us  [local(): pl.pallas_call(functools.partial(mix_kernel, hidden.shape[1] * n_tp, inne...]
    concatenate x0 -> x1, local copies, waits for them, and re-layouts: none -> 1.46 us  [local(): jnp.concatenate([product, fill], axis=1).reshape(n_tp, rows, -1)]
    convert_element_type x1 -> x0, other arithmetic: 1.45 us -> none  [local(): mixed = (norm * summed[:, :block].astype(jnp.float32)).astype(jnp.bfloat16)]
    pallas_call x1, Pallas kernels: 10.1 us -> 11.5 us  [local(): pl.pallas_call(state_kernel, out_shape=jax.ShapeDtypeStruct(saved_states....]
  transfers between devices with their start and end apart: 2 -> 0, of which waited for: 2 -> 0; matrix products, arithmetic and copies ran while one was open for 0% -> 0% of each run, Pallas kernels for 8% -> 0%
where the time goes in v2:
time: 59.8 us; the launch traced here: 58.9 us
  Pallas kernels  47.8 us (80%)
  matrix products  5.59 us (9%)
  local copies, waits for them, and re-layouts  3.01 us (5%)
  other arithmetic  1.83 us (3%)
  between operations  0.68 us (1%)
    pallas_call x2, Pallas kernels, exchange_call(): pl.pallas_call(body, out_shape=out_shape, in_specs=[pl.BlockSpec(memory_s...  27.1 us
    pallas_call x1, Pallas kernels, local(): pl.pallas_call(state_kernel, out_shape=jax.ShapeDtypeStruct(saved_states....  11.5 us
    pallas_call x1, Pallas kernels, local(): pl.pallas_call(functools.partial(mix_kernel, hidden.shape[1] * n_tp, inne...  9.18 us
    dot_general x1, matrix products, local(): jnp.dot(entry, weights, preferred_element_type=jnp.float32)  5.59 us
    unnamed x4, local copies, waits for them, and re-layouts  1.54 us
    concatenate x1, local copies, waits for them, and re-layouts, local(): jnp.concatenate([product, fill], axis=1).reshape(n_tp, rows, -1)  1.46 us

profile of v2, /device:TPU:0, one launch (start us, length us, event | category | flops | bytes accessed | tf_op | source)
XLA Modules:
  0.0 58.9 jit_solution(17094234568084997740)
XLA Ops:
  0.6 1.1 %fusion.12 = bf16[128]{0:T(256)(128)(2,1)S(1)} fusion(bf16[128,1024]{1,0:T(8,128)(2,1)} %param.17), kind=kLoop, calls=%fused_computation.13 | loop fusion | flops 393088 | bytes 262400 | tf_op jit(solution)/shard_map/reduce_sum | solution.py:412
  1.7 0.7 %convert_element_type.21 = f32[1024]{0:T(1024)S(1)} convert(bf16[1024]{0:T(1024)(128)(2,1)} %param.18) | non-fusion elementwise | flops 1024 | bytes 6144 | tf_op jit(solution)/shard_map/convert_element_type | solution.py:413
  2.4 0.9 %copy.21 = bf16[1024,16]{1,0:T(8,128)(2,1)S(1)} copy(bf16[1024,16]{0,1:T(8,128)(2,1)} %param.22) | data formatting | bytes 65536 | tf_op args[5]
  3.3 5.6 %fusion.8 = bf16[128,3088]{0,1:T(8,128)(2,1)S(1)} fusion(bf16[1024,16]{1,0:T(8,128)(2,1)S(1)} %copy.21, bf16[1024,1024]{1,0:T(8,128)(2,1)} %param.21, bf16[1024,1024]{1,0:T(8,128)(2,1)} %param.20, bf16[1024,1024]{1,0:T(8,128)(2,1)} %param.19, bf16[128,1024]{1,0:T(8,128)(2,1)} %param.17, f32[1024]{0:T(1024)S(1)} %convert_element_type.21), kind=kOutput, calls=%fused_computation.8 | convolution fusion | flops 835586048 | bytes 7380992 | tf_op jit(solution)/shard_map/dot_general | solution.py:415
  8.9 0.1 pad_maximum_fusion
  9.0 1.5 %copy.22 = bf16[128,3200]{1,0:T(8,128)(2,1)} copy(bf16[128,3200]{0,1:T(8,128)(2,1)S(1)} %pad_maximum_fusion) | data formatting | bytes 1638400 | tf_op jit(solution)/shard_map/concatenate | solution.py:419
  10.5 14.2 %entry_exchange.1.proj_ref = f32[32,3200]{1,0:T(8,128)} custom-call(bf16[4,32,3200]{2,1,0:T(8,128)(2,1)} %bitcast.5), custom_call_target="tpu_custom_call" | custom-call | tf_op jit(solution)/shard_map/entry_exchange/pallas_call | solution.py:384
  24.7 9.2 %mix.1 = (bf16[8,32,640]{2,1,0:T(8,128)(2,1)}, bf16[7,8,1024]{2,1,0:T(8,128)(2,1)}, bf16[7,8,1024]{2,1,0:T(8,128)(2,1)}, bf16[32,1024]{1,0:T(8,128)(2,1)}, bf16[32,512]{1,0:T(8,128)(2,1)}, /*index=5*/f32[32,128]{1,0:T(8,128)}) custom-call(s32[8]{0:T(128)} %acc_smem.3, f32[16]{0:T(128)} %bias_smem.1, f32[16]{0:T(128)} %decay_smem.1, f32[16]{0:T(128)} %skip_smem.1, ...), custom_call_target="tpu_custom_call" | custom-call | flops 268435456 | bytes 14680064 | tf_op jit(solution)/shard_map/mix/pallas_call | solution.py:426
  33.9 12.9 %exit_exchange.1 = bf16[32,512]{1,0:T(8,128)(2,1)} custom-call(bf16[8,32,640]{2,1,0:T(8,128)(2,1)} %get-tuple-element.10.blocks_ref), custom_call_target="tpu_custom_call" | custom-call | tf_op jit(solution)/shard_map/exit_exchange/pallas_call | solution.py:384
  46.8 0.0 copy-start
  46.8 11.5 %states.1 = f32[8,5,16,64,128]{4,3,2,1,0:T(8,128)} custom-call(s32[8]{0:T(128)} %acc_smem.3, f32[32,128]{1,0:T(8,128)} %get-tuple-element.11.a_smem, bf16[32,1024]{1,0:T(8,128)(2,1)} %get-tuple-element.12.xdt_ref, bf16[32,512]{1,0:T(8,128)(2,1)} %get-tuple-element.13.b_ref, f32[8,5,16,64,128]{4,3,2,1,0:T(8,128)} %s0_ref.1), custom_call_target="tpu_custom_call" | custom-call | flops 10485760 | bytes 31457280 | tf_op jit(solution)/shard_map/states/pallas_call | solution.py:457
  58.3 0.0 copy-done
  58.3 0.6 %copy.24 = bf16[32,512]{1,0:T(8,128)(2,1)} copy(bf16[32,512]{1,0:T(8,128)(2,1)S(1)} %copy-done) | data formatting | bytes 65536
  (1 shorter events, 0.0 us)
Async XLA Ops:
  46.8 11.5 %copy-start = (bf16[32,512]{1,0:T(8,128)(2,1)S(1)}, bf16[32,512]{1,0:T(8,128)(2,1)}, u32[]{:S(2)}) copy-start(bf16[32,512]{1,0:T(8,128)(2,1)} %exit_exchange.1) | copy-start | bytes 98308
